TPU v7x, 256 devices: a 4x2x16 block of a 4x16x16 slice. The times are simulated.
256 devices in a mesh: grp: 2 (over y), ep: 32 (over z, core), tp: 4 (over x).
Axes of the slice: x: 4, y: 2, z: 16, core: 2. Of those that a mesh axis runs over, the one named last changes fastest.
The devices are a block of a 4x16x16 slice.
Arguments:
- tokens: bfloat16 [16384, 2048], P(('grp', 'ep', 'tp')), parts along dimension 0, may hold values from -6 to 6
- gain_in: float32 [2048], replicated, may hold values from 0.1 to 1.9
- routes: int32 [16384, 2], P(('grp', 'ep')), parts along dimension 0, may hold values from 0 to 31, all different within a row; in each aligned block of 64 rows (0 to 63, 64 to 127, ...) at most 6 rows name the same one
- gates: float32 [16384, 2], P(('grp', 'ep')), parts along dimension 0, may hold values from 0.05 to 1
- w_gate: bfloat16 [32, 2048, 3072], P('ep', None, 'tp'), may hold values from -0.125 to 0.125
- w_up: bfloat16 [32, 2048, 3072], P('ep', None, 'tp'), may hold values from -0.125 to 0.125
- w_down: bfloat16 [32, 3072, 2048], P('ep', 'tp'), may hold values from -0.109375 to 0.109375
- gain_out: float32 [2048], P('tp'), may hold values from 0.3 to 3
Outputs:
- mixed: bfloat16 [16384, 2048], P(('grp', 'ep'), 'tp'), parts along dimension 0
There are 2 independent parts, one for each index of `grp`. A program takes and returns all parts, laid end to end along the dimension named above; an argument that names none is the same for every part. Nothing has to cross between parts.
Inputs may be any that keep to these rules, and one draw needn't show every extreme that they name: `routes`: each row names 2 different experts; every expert is named by some row. Among the rows of one device (aligned blocks of 64 rows) no expert is named more than 6 times, and in every draw some expert is named exactly 6 times in some such block.
All inputs are finite; a program needn't handle non-finite values.
Results may differ from a plain program's by a relative error of at most 0.012.
Values may be sent and summed in bfloat16 or wider, within the bound.
A program may use at most 64 MiB of HBM per device.

v0:
```python
import jax
import jax.numpy as jnp
from jax import lax
from jax.sharding import PartitionSpec as P

EPS = 1e-06


def from_everyone(shard, axis):
    size = lax.axis_size(axis)
    return lax.all_to_all(
        jnp.broadcast_to(shard[None], (size, *shard.shape)), axis, 0, 0, tiled=True
    )


def of_everyone(shard, axis):
    everything = from_everyone(shard, axis)
    return jnp.sum(everything, axis=0)


def slot_table(routes, experts, capacity):
    sources, count, choose = routes.shape
    flat = routes.reshape(sources, count * choose)
    onehot = (flat[:, :, None] == jnp.arange(experts, dtype=jnp.int32)[None, None, :]).astype(
        jnp.int32
    )
    earlier = jnp.cumsum(onehot, axis=1) - onehot
    slot = jnp.sum(earlier * onehot, axis=2)
    return (flat * capacity + slot).reshape(sources, count, choose)


def local(tokens, gain_in, routes, gates, w_gate, w_up, w_down, gain_out):
    count, width = tokens.shape
    choose = routes.shape[1]
    experts = lax.axis_size("ep")
    groups = lax.axis_size("tp")
    capacity = (3 * count * choose + 2 * experts - 1) // (2 * experts)
    hidden_width = w_gate.shape[2]
    values = tokens.astype(jnp.float32)
    normed = (
        values * lax.rsqrt(jnp.mean(values * values, axis=-1, keepdims=True) + EPS) * gain_in
    ).astype(jnp.bfloat16)
    positions = slot_table(routes.reshape(groups, count, choose), experts, capacity)
    own = lax.dynamic_index_in_dim(positions, lax.axis_index("tp"), 0, keepdims=False)
    slots = jnp.arange(experts * capacity, dtype=jnp.int32)
    select = jnp.sum((own[None, :, :] == slots[:, None, None]).astype(jnp.bfloat16), axis=2)
    outgoing = jnp.dot(select, normed, preferred_element_type=jnp.float32).astype(jnp.bfloat16)
    outgoing = outgoing.reshape(experts, capacity, width)
    arrived = lax.all_to_all(outgoing, "ep", split_axis=0, concat_axis=0, tiled=True)
    piece = lax.all_gather(arrived[:, None], "tp", axis=1, tiled=True)
    flat = piece.reshape(-1, width)
    gate = jnp.dot(flat, w_gate[0], preferred_element_type=jnp.float32)
    up = jnp.dot(flat, w_up[0], preferred_element_type=jnp.float32)
    hidden = (jax.nn.silu(gate) * up).astype(jnp.bfloat16)
    hidden = hidden.reshape(piece.shape[:-1] + (hidden_width,))
    partial_value = jnp.dot(
        hidden.reshape(-1, hidden_width), w_down[0], preferred_element_type=jnp.float32
    )
    summed = lax.psum_scatter(
        partial_value.astype(jnp.bfloat16), "tp", scatter_dimension=1, tiled=True
    )
    slice_width = width // groups
    expert_out = summed.reshape(experts, groups * capacity, slice_width)
    returned = lax.all_to_all(expert_out, "ep", split_axis=0, concat_axis=0, tiled=True)
    returned = returned.reshape(experts, groups, capacity, slice_width).transpose(1, 0, 2, 3)
    returned = returned.reshape(groups, experts * capacity, slice_width).astype(jnp.float32)
    weights = gates.reshape(groups, count, choose)
    combine = jnp.sum(
        jnp.where(
            positions[..., None] == slots[None, None, None, :], weights[..., None], jnp.float32(0.0)
        ),
        axis=2,
    )
    combined = jnp.einsum("gtp,gpd->gtd", combine, returned)
    combined = combined.reshape(groups * count, slice_width)
    squares = of_everyone(jnp.sum(combined * combined, axis=1), "tp")
    scale = lax.rsqrt(squares / width + EPS)
    return (combined * scale[:, None] * gain_out).astype(jnp.bfloat16)


def solution(mesh):
    in_specs = (
        P(("grp", "ep", "tp"), None),
        P(),
        P(("grp", "ep"), None),
        P(("grp", "ep"), None),
        P("ep", None, "tp"),
        P("ep", None, "tp"),
        P("ep", "tp", None),
        P("tp"),
    )
    out_specs = P(("grp", "ep"), "tp")
    return jax.shard_map(local, mesh=mesh, in_specs=in_specs, out_specs=out_specs, check_vma=False)
```

profile of v0, /device:TPU:33, one launch (start us, length us, event | category | flops | bytes accessed | tf_op | source)
XLA Modules:
  0.0 278.8 jit_solution(4888810411502820431)
XLA Ops:
  6.6 1.0 copy.61
  7.5 0.7 broadcast_multiply_fusion
  8.2 0.1 eq.43
  8.3 0.8 fusion.19
  9.2 1.2 reduce_window_sum.11
  10.4 0.2 select_reduce_fusion.1
  10.7 0.1 copy.62
  10.8 0.1 copy.63
  10.9 0.1 mul.65
  11.0 0.1 fusion.21
  11.1 1.1 fusion.11
  12.2 2.3 convolution_convert_fusion.1
  14.5 2.2 reshape.60
  16.7 80.9 %all_to_all.16 = bf16[32,6,2048]{2,1,0:T(8,128)(2,1)S(1)} all-to-all(bf16[32,6,2048]{2,1,0:T(8,128)(2,1)} %reshape.60), channel_id=1, replica_groups=mesh['grp'=2,'ep'=32,'tp'=4] {'ep'}, dimensions={0} | all-to-all | bytes 1572864 | tf_op jit(solution)/shard_map/all_to_all | solution.py:49
  97.6 1.3 copy.66
  99.0 0.1 reduce-scatter.2.cloned.1.call-start
  99.1 38.0 %all-gather.3.cloned.1.call-done = bf16[32,24,2048]{2,0,1:T(8,128)(2,1)} async-done(((bf16[32,6,2048]{2,0,1:T(8,128)(2,1)}), bf16[32,24,2048]{2,0,1:T(8,128)(2,1)}) %all-gather.3.cloned.1.call-update) | async-done | bytes 3145744 | tf_op jit(solution)/shard_map/all_gather | solution.py:50
  137.1 3.8 %copy.67 = bf16[32,24,2048]{2,1,0:T(8,128)(2,1)S(1)} copy(bf16[32,24,2048]{2,0,1:T(8,128)(2,1)} %all-gather.3.cloned.1.call-done) | data formatting | bytes 6291456 | tf_op jit(solution)/shard_map/all_gather | solution.py:50
  140.9 1.7 copy-done.1
  142.6 4.0 %fusion.1 = f32[768,768]{1,0:T(8,128)} fusion(bf16[768,2048]{1,0:T(8,128)(2,1)S(1)} %bitcast.35, bf16[1,2048,768]{2,1,0:T(8,128)(2,1)S(1)} %copy-done.4), kind=kOutput, calls=%fused_computation.2 | convolution fusion | flops 2415919104 | bytes 8650752 | tf_op jit(solution)/shard_map/dot_general | solution.py:53
  146.6 11.0 %convolution_convert_fusion = bf16[768,2048]{1,0:T(8,128)(2,1)} fusion(bf16[1,768,2048]{2,1,0:T(8,128)(2,1)S(1)} %copy-done, f32[768,768]{1,0:T(8,128)} %fusion.1, bf16[768,2048]{1,0:T(8,128)(2,1)} %bitcast.36, bf16[1,2048,768]{2,1,0:T(8,128)(2,1)} %param.12), kind=kOutput, calls=%fused_computation | convolution fusion | flops 4836950016 | bytes 14942208 | tf_op jit(solution)/shard_map/dot_general | solution.py:56
  157.7 44.8 %reduce-scatter.2.cloned.1.call-done = bf16[768,512]{1,0:T(8,128)(2,1)} async-done(((bf16[768,2048]{1,0:T(8,128)(2,1)}), bf16[768,512]{1,0:T(8,128)(2,1)}) %reduce-scatter.2.cloned.1.call-update) | async-done | bytes 786448 | tf_op jit(solution)/shard_map/reduce_scatter | solution.py:59
  202.5 13.3 %all-to-all-start.1 = ((bf16[32,24,512]{2,1,0:T(8,128)(2,1)}), bf16[32,24,512]{2,1,0:T(8,128)(2,1)}, u32[]{:S(2)}, u32[]{:S(2)}) async-start(bf16[32,24,512]{2,1,0:T(8,128)(2,1)} %bitcast.39), calls=%async_computation.2 | async-start | bytes 1572864 | tf_op jit(solution)/shard_map/all_to_all | solution.py:64
  215.8 0.1 broadcast_in_dim.20
  215.9 0.2 select_reduce_fusion
  216.1 44.2 %all-to-all-done.1 = bf16[32,24,512]{2,1,0:T(8,128)(2,1)} async-done(((bf16[32,24,512]{2,1,0:T(8,128)(2,1)}), bf16[32,24,512]{2,1,0:T(8,128)(2,1)}, u32[]{:S(2)}, u32[]{:S(2)}) %all-to-all-start.1) | async-done | bytes 786464 | tf_op jit(solution)/shard_map/all_to_all | solution.py:64
  260.3 1.4 copy.68
  261.7 0.6 copy.69
  262.3 1.1 multiply_reduce_fusion
  263.4 0.1 broadcast_in_dim.37
  263.5 6.5 %all_to_all.17 = f32[4,1,256]{2,1,0:T(1,128)S(1)} all-to-all(f32[4,1,256]{2,1,0:T(1,128)S(1)} %broadcast_in_dim.38), channel_id=1, replica_groups=mesh['grp'=2,'ep'=32,'tp'=4] {'tp'}, dimensions={0} | all-to-all | bytes 8192 | tf_op jit(solution)/shard_map/all_to_all | solution.py:11
  270.1 1.9 fusion.15
  (20 shorter events, 0.2 us)
Async XLA Ops:
  6.5 140.1 %copy-start = (bf16[1,768,2048]{2,1,0:T(8,128)(2,1)S(1)}, bf16[1,768,2048]{2,1,0:T(8,128)(2,1)}, u32[]{:S(2)}) copy-start(bf16[1,768,2048]{2,1,0:T(8,128)(2,1)} %param.14) | copy-start | bytes 9437188
  6.6 130.6 %all-gather.3.cloned.1.call-start = ((), (), s32[]{:S(2)}) async-start(), calls=%async_computation.5 | async-start | bytes 3932160 | tf_op jit(solution)/shard_map/all_gather | solution.py:50
  99.0 103.5 %reduce-scatter.2.cloned.1.call-start = ((), (), s32[]{:S(2)}) async-start(), calls=%async_computation.4 | async-start | bytes 3932160 | tf_op jit(solution)/shard_map/reduce_scatter | solution.py:59
  137.1 5.5 %copy-start.4 = (bf16[1,2048,768]{2,1,0:T(8,128)(2,1)S(1)}, bf16[1,2048,768]{2,1,0:T(8,128)(2,1)}, u32[]{:S(2)}) copy-start(bf16[1,2048,768]{2,1,0:T(8,128)(2,1)} %param.13) | copy-start | bytes 9437188
  140.9 1.7 copy-start.1
  157.6 58.2 %copy-start.3 = (f32[256,2]{0,1:T(2,128)S(1)}, f32[256,2]{0,1:T(2,128)}, u32[]{:S(2)}) copy-start(f32[256,2]{0,1:T(2,128)} %param.11) | copy-start | bytes 6148
  202.5 67.6 %copy-start.2 = (f32[512]{0:T(512)S(1)}, f32[512]{0:T(512)}, u32[]{:S(2)}) copy-start(f32[512]{0:T(512)} %param.15) | copy-start | bytes 6148
  202.5 57.8 %all-to-all-start.1 = ((bf16[32,24,512]{2,1,0:T(8,128)(2,1)}), bf16[32,24,512]{2,1,0:T(8,128)(2,1)}, u32[]{:S(2)}, u32[]{:S(2)}) async-start(bf16[32,24,512]{2,1,0:T(8,128)(2,1)} %bitcast.39), calls=%async_computation.2 | async-start | bytes 1572864 | tf_op jit(solution)/shard_map/all_to_all | solution.py:64
Sparse Core Ops, SparseCore 0:
  99.1 37.9 all-gather.2
  157.8 44.6 reduce-scatter.1
where the time goes:
time: 279 us
  waiting for transfers between devices  127 us (46%)
  blocking collectives  87.4 us (31%)
  matrix products  18.5 us (7%)
  between operations  13.5 us (5%)
  starting transfers between devices  13.4 us (5%)
  local copies, waits for them, and re-layouts  12.5 us (4%)
  other arithmetic  6.3 us (2%)
    all_to_all x1, blocking collectives, local(): lax.all_to_all(outgoing, 'ep', split_axis=0, concat_axis=0, tiled=True)  80.9 us
    reduce_scatter x1, waiting for transfers between devices, local(): lax.psum_scatter(partial_value.astype(jnp.bfloat16), 'tp', scatter_dimens...  44.8 us
    all_to_all x1, waiting for transfers between devices, local(): lax.all_to_all(expert_out, 'ep', split_axis=0, concat_axis=0, tiled=True)  44.2 us
    all_gather x1, waiting for transfers between devices, local(): piece = lax.all_gather(arrived[:, None], 'tp', axis=1, tiled=True)  38 us
    all_to_all x1, starting transfers between devices, local(): lax.all_to_all(expert_out, 'ep', split_axis=0, concat_axis=0, tiled=True)  13.3 us
    dot_general x1, matrix products, local(): jnp.dot(hidden.reshape(-1, hidden_width), w_down[0], preferred_element_ty...  11 us
    all_to_all x1, blocking collectives, from_everyone(): lax.all_to_all(jnp.broadcast_to(shard[None], (size, *shard.shape)), axis,...  6.5 us
  transfers between devices with their start and end apart: 3, of which 3 were waited for; matrix products, arithmetic and copies ran while one was open for 0% of the time, Pallas kernels for 0%

commit v1 on v0

v1 whole, which is shorter than its diff:
```python
import functools

import jax
import jax.numpy as jnp
from jax import lax
from jax.experimental import pallas as pl
from jax.experimental.pallas import tpu as pltpu
from jax.sharding import PartitionSpec as P

EPS = 1e-06
MESH = pl.DeviceIdType.MESH
BF = jnp.bfloat16
F32 = jnp.float32


def layer_kernel(
    experts, groups, cap,
    tokens_ref, gain_ref, routes_ref, gates_ref, wg_hbm, wu_hbm, wd_hbm, gout_ref,
    out_ref,
    wg, wu, wd, piece, column, select, slots, rows, hidden, partial, terms, result, answers, comb_hi, comb_lo, squares,
    w_sem, xa_s, xa_r, zs_s, zs_r, ag_s, ag_r, rs_s, rs_r, zr_s, zr_r, sq_s, sq_r,
):
    grp, ep, tp = lax.axis_index("grp"), lax.axis_index("ep"), lax.axis_index("tp")
    z, c = ep // 2, ep % 2
    nz = experts // 2
    count, width = tokens_ref.shape
    local_tokens = groups * count
    slice_width = width // groups
    block = groups * cap
    per_chunk = 4
    chunks = experts // per_chunk
    chunk_rows = per_chunk * block
    hidden_width = wg.shape[1]

    def offsets(k):
        far = jnp.where(k == 0, 1, nz // 2 + 1 - k)
        return jnp.where(k == 1, 0, far), jnp.where(k == 1, nz // 2, nz - far)

    def expert_at(k, j):
        first, second = offsets(k)
        d = first if j < 2 else second
        return ((z + d) % nz) * 2 + (c + j % 2) % 2

    def source_at(k, j):
        first, second = offsets(k)
        d = first if j < 2 else second
        return ((z + nz - d) % nz) * 2 + (c + j % 2) % 2

    def peer(j):
        return (tp + j) % groups

    def giver(j):
        return (tp + groups - j) % groups

    barrier = pltpu.get_barrier_semaphore()
    for j in range(1, groups):
        pl.semaphore_signal(barrier, inc=1, device_id=(grp, ep, peer(j)), device_id_type=MESH)

    def greet(i, carry):
        pl.semaphore_signal(barrier, inc=1, device_id=(grp, (ep + i) % experts, tp), device_id_type=MESH)
        return carry

    lax.fori_loop(1, experts, greet, 0)

    w_copies = [
        pltpu.make_async_copy(src.at[0], dst, w_sem.at[i])
        for i, (src, dst) in enumerate(((wg_hbm, wg), (wu_hbm, wu), (wd_hbm, wd)))
    ]
    for copy in w_copies:
        copy.start()

    values = tokens_ref[...].astype(F32)
    normed = values * lax.rsqrt(jnp.mean(values * values, axis=-1, keepdims=True) + EPS) * gain_ref[...]
    normed = normed.astype(BF)
    for q in range(groups):
        piece[q] = normed[:, q * slice_width:(q + 1) * slice_width]

    at = lax.broadcasted_iota(jnp.int32, (experts, local_tokens), 0)
    k_of, j_of = at // per_chunk, at % per_chunk
    first, second = offsets(k_of)
    d_of = jnp.where(j_of < 2, first, second)
    expert = ((z + d_of) % nz) * 2 + (c + j_of % 2) % 2
    hit0 = routes_ref[0:1, :] == expert
    hit1 = routes_ref[1:2, :] == expert
    zero = jnp.zeros((), F32)
    one = jnp.ones((), F32)
    hit = jnp.where(hit0, one, zero) + jnp.where(hit1, one, zero)
    before = (
        lax.broadcasted_iota(jnp.int32, (local_tokens, local_tokens), 0)
        < lax.broadcasted_iota(jnp.int32, (local_tokens, local_tokens), 1)
    )
    before = jnp.where(before, one, zero).astype(BF)
    rank = jnp.dot(hit.astype(BF), before, preferred_element_type=F32)
    rank = jnp.where(hit > 0, rank, -one)
    gate = jnp.where(hit0, gates_ref[0:1, :], zero) + jnp.where(hit1, gates_ref[1:2, :], zero)
    slot_of = lax.broadcasted_iota(jnp.int32, (experts, block, local_tokens), 1).astype(F32)
    chosen = rank[:, None, :] == slot_of
    select[...] = jnp.where(chosen, one, zero).reshape(experts * block, local_tokens).astype(BF)

    pl.semaphore_wait(barrier, groups - 1 + experts - 1)

    def xa_copy(j, src, dst, device):
        return pltpu.make_async_remote_copy(
            src_ref=piece.at[src], dst_ref=column.at[dst], send_sem=xa_s.at[j - 1], recv_sem=xa_r.at[j - 1],
            device_id=(grp, ep, device), device_id_type=MESH)

    for j in range(1, groups):
        xa_copy(j, peer(j), tp, peer(j)).start()
    column[tp] = piece[tp]
    for j in range(1, groups):
        xa_copy(j, peer(j), giver(j), peer(j)).wait_recv()

    def zs_copy(k, j):
        pos = k * per_chunk + j
        return pltpu.make_async_remote_copy(
            src_ref=slots.at[pos], dst_ref=rows.at[tp, pos], send_sem=zs_s.at[pos], recv_sem=zs_r.at[pos],
            device_id=(grp, expert_at(k, j), tp), device_id_type=MESH)

    def each(k, action):
        for j in range(per_chunk):
            if j == 0:
                @pl.when(k != 1)
                def _():
                    action(j)
            else:
                action(j)

    features = column[...].reshape(local_tokens, slice_width)

    def dispatch(k, carry):
        picked = jnp.dot(
            select[pl.ds(pl.multiple_of(k * chunk_rows, chunk_rows), chunk_rows), :],
            features, preferred_element_type=F32)
        slots[pl.ds(k * per_chunk, per_chunk)] = picked.reshape(per_chunk, block, slice_width).astype(BF)
        each(k, lambda j: zs_copy(k, j).start())
        return carry

    lax.fori_loop(0, chunks, dispatch, 0)
    rows[tp, per_chunk] = slots[per_chunk]

    high = gate.astype(BF).astype(F32)
    low = gate - high
    comb_hi[...] = jnp.where(chosen, high[:, None, :], zero).reshape(experts * block, local_tokens).T.astype(BF)
    comb_lo[...] = jnp.where(chosen, low[:, None, :], zero).reshape(experts * block, local_tokens).T.astype(BF)

    for copy in w_copies:
        copy.wait()

    def span(k):
        return pl.ds(k * per_chunk, per_chunk)

    def ag_copy(k, j, owner):
        i = k * (groups - 1) + j - 1
        return pltpu.make_async_remote_copy(
            src_ref=rows.at[tp, span(k)], dst_ref=rows.at[owner, span(k)], send_sem=ag_s.at[i], recv_sem=ag_r.at[i],
            device_id=(grp, ep, peer(j)), device_id_type=MESH)

    def rs_copy(k, j, owner):
        i = k * (groups - 1) + j - 1
        return pltpu.make_async_remote_copy(
            src_ref=partial.at[peer(j), span(k)], dst_ref=terms.at[owner, span(k)],
            send_sem=rs_s.at[i], recv_sem=rs_r.at[i],
            device_id=(grp, ep, peer(j)), device_id_type=MESH)

    def zr_copy(k, j):
        pos = k * per_chunk + j
        return pltpu.make_async_remote_copy(
            src_ref=result.at[pos], dst_ref=answers.at[pos], send_sem=zr_s.at[pos], recv_sem=zr_r.at[pos],
            device_id=(grp, source_at(k, j), tp), device_id_type=MESH)

    def gather(k):
        each(k, lambda j: zs_copy(k, j).wait_recv())
        for j in (1, 3, 2):
            ag_copy(k, j, tp).start()

    def compute(k):
        for j in range(1, groups):
            ag_copy(k, j, giver(j)).wait_recv()
        x = jnp.concatenate(
            [rows[q, span(k)].reshape(chunk_rows, slice_width) for q in range(groups)], axis=1)
        step = 256
        for n in range(hidden_width // step):
            cols = slice(n * step, (n + 1) * step)
            g = jnp.dot(x, wg[:, cols], preferred_element_type=F32)
            u = jnp.dot(x, wu[:, cols], preferred_element_type=F32)
            hidden[:, cols] = (g * (1.0 / (1.0 + jnp.exp(-g))) * u).astype(BF)
        h = hidden[...]
        for j in (1, 3, 2, 0):
            q = peer(j)
            part = jnp.dot(
                h, wd[:, pl.ds(pl.multiple_of(q * slice_width, slice_width), slice_width)],
                preferred_element_type=F32)
            partial[q, span(k)] = part.reshape(per_chunk, block, slice_width).astype(BF)
            if j != 0:
                rs_copy(k, j, tp).start()

    def give_back(k):
        for j in range(1, groups):
            rs_copy(k, j, giver(j)).wait_recv()
        total = partial[tp, span(k)].astype(F32)
        for j in range(1, groups):
            total += terms[giver(j), span(k)].astype(F32)
        result[span(k)] = total.astype(BF)
        each(k, lambda j: zr_copy(k, j).start())

    def pipeline(s, carry):
        @pl.when(s < chunks)
        def _():
            gather(s)

        @pl.when((s >= 1) & (s <= chunks))
        def _():
            compute(s - 1)

        @pl.when(s >= 2)
        def _():
            give_back(s - 2)
        return carry

    lax.fori_loop(0, chunks + 2, pipeline, 0)
    answers[per_chunk] = result[per_chunk]

    def collect(k, carry):
        each(k, lambda j: zr_copy(k, j).wait_recv())
        return carry

    lax.fori_loop(0, chunks, collect, 0)
    outs = answers[...].reshape(experts * block, slice_width)
    combined = jnp.dot(comb_hi[...], outs, preferred_element_type=F32)
    combined += jnp.dot(comb_lo[...], outs, preferred_element_type=F32)

    own = jnp.sum(combined * combined, axis=1, keepdims=True)
    squares[tp] = jnp.broadcast_to(own, (local_tokens, 128)).T[:8]

    def sq_copy(j, owner):
        return pltpu.make_async_remote_copy(
            src_ref=squares.at[tp], dst_ref=squares.at[owner], send_sem=sq_s.at[j - 1], recv_sem=sq_r.at[j - 1],
            device_id=(grp, ep, peer(j)), device_id_type=MESH)

    for j in range(1, groups):
        sq_copy(j, tp).start()
    for j in range(1, groups):
        sq_copy(j, giver(j)).wait_recv()
    total = squares[0] + squares[1] + squares[2] + squares[3]
    scale = lax.rsqrt(total / width + EPS)
    scale = jnp.concatenate([scale] * 16, axis=0).T[:, :1]
    out_ref[...] = (combined * scale * gout_ref[...]).astype(BF)

    def drain(k, carry):
        each(k, lambda j: zs_copy(k, j).wait_send())
        each(k, lambda j: zr_copy(k, j).wait_send())
        for j in range(1, groups):
            ag_copy(k, j, tp).wait_send()
            rs_copy(k, j, tp).wait_send()
        return carry

    lax.fori_loop(0, chunks, drain, 0)
    for j in range(1, groups):
        xa_copy(j, peer(j), tp, peer(j)).wait_send()
        sq_copy(j, tp).wait_send()


def local(tokens, gain_in, routes, gates, w_gate, w_up, w_down, gain_out):
    count, width = tokens.shape
    choose = routes.shape[1]
    experts = lax.axis_size("ep")
    groups = lax.axis_size("tp")
    cap = (3 * count * choose + 2 * experts - 1) // (2 * experts)
    hidden_width = w_gate.shape[2]
    slice_width = width // groups
    block = groups * cap
    tokens_here = groups * count
    chunks = experts // 4
    vmem = pl.BlockSpec(memory_space=pltpu.VMEM)
    hbm = pl.BlockSpec(memory_space=pl.ANY)
    dma = pltpu.SemaphoreType.DMA
    return pl.pallas_call(
        functools.partial(layer_kernel, experts, groups, cap),
        out_shape=jax.ShapeDtypeStruct((tokens_here, slice_width), BF),
        in_specs=[vmem, vmem, vmem, vmem, hbm, hbm, hbm, vmem],
        out_specs=vmem,
        scratch_shapes=[
            pltpu.VMEM((width, hidden_width), BF),
            pltpu.VMEM((width, hidden_width), BF),
            pltpu.VMEM((hidden_width, width), BF),
            pltpu.VMEM((groups, count, slice_width), BF),
            pltpu.VMEM((groups, count, slice_width), BF),
            pltpu.VMEM((experts * block, tokens_here), BF),
            pltpu.VMEM((experts, block, slice_width), BF),
            pltpu.VMEM((groups, experts, block, slice_width), BF),
            pltpu.VMEM((4 * block, hidden_width), BF),
            pltpu.VMEM((groups, experts, block, slice_width), BF),
            pltpu.VMEM((groups, experts, block, slice_width), BF),
            pltpu.VMEM((experts, block, slice_width), BF),
            pltpu.VMEM((experts, block, slice_width), BF),
            pltpu.VMEM((tokens_here, experts * block), BF),
            pltpu.VMEM((tokens_here, experts * block), BF),
            pltpu.VMEM((groups, 8, tokens_here), F32),
            dma((3,)),
            dma((groups - 1,)), dma((groups - 1,)),
            dma((experts,)), dma((experts,)),
            dma((chunks * (groups - 1),)), dma((chunks * (groups - 1),)),
            dma((chunks * (groups - 1),)), dma((chunks * (groups - 1),)),
            dma((experts,)), dma((experts,)),
            dma((groups - 1,)), dma((groups - 1,)),
        ],
        compiler_params=pltpu.CompilerParams(
            collective_id=0, has_side_effects=True, vmem_limit_bytes=56 * 1024 * 1024),
        name="routed_experts",
    )(tokens, gain_in.reshape(1, width), routes.T, gates.T, w_gate, w_up, w_down, gain_out.reshape(1, slice_width))


def solution(mesh):
    in_specs = (
        P(("grp", "ep", "tp"), None),
        P(),
        P(("grp", "ep"), None),
        P(("grp", "ep"), None),
        P("ep", None, "tp"),
        P("ep", None, "tp"),
        P("ep", "tp", None),
        P("tp"),
    )
    out_specs = P(("grp", "ep"), "tp")
    return jax.shard_map(local, mesh=mesh, in_specs=in_specs, out_specs=out_specs, check_vma=False)
```

time: 279 us -> 133 us (0.48)
  the two profiles are of different devices: /device:TPU:33 before, /device:TPU:160 now
where the time goes in v1:
time: 133 us; the launch traced here: 132 us
  Pallas kernels  131 us (98%)
  local copies, waits for them, and re-layouts  1.67 us (1%)
    pallas_call x1, Pallas kernels, local(): pl.pallas_call(functools.partial(layer_kernel, experts, groups, cap), out...  131 us

profile of v1, /device:TPU:160, one launch (start us, length us, event | category | flops | bytes accessed | tf_op | source)
XLA Modules:
  0.0 132.5 jit_solution(18323109879234768533)
XLA Ops:
  0.0 130.8 %routed_experts.1 = bf16[256,512]{1,0:T(8,128)(2,1)} custom-call(bf16[64,2048]{1,0:T(8,128)(2,1)} %tokens_ref.1, f32[1,2048]{1,0:T(1,128)} %bitcast.4, s32[2,256]{1,0:T(2,128)} %bitcast.5, f32[2,256]{1,0:T(2,128)} %bitcast.6, bf16[1,2048,768]{2,1,0:T(8,128)(2,1)} %wg_hbm.1, bf16[1,2048,768]{2,1,0:T(8,128)(2,1)} %wu_hbm.1, bf16[1,768,2048]{2,1,0:T(8,128)(2,1)} %wd_hbm.1, ...), custom_call_target="tpu_custom_call" | custom-call | tf_op jit(solution)/shard_map/routed_experts/pallas_call | solution.py:277
  130.8 1.7 %copy.10 = bf16[256,512]{1,0:T(8,128)(2,1)} copy(bf16[256,512]{1,0:T(8,128)(2,1)} %routed_experts.1) | data formatting | bytes 524288

commit v2 on v1

v2 whole, which is shorter than its diff:
```python
import functools

import jax
import jax.numpy as jnp
from jax import lax
from jax.experimental import pallas as pl
from jax.experimental.pallas import tpu as pltpu
from jax.sharding import PartitionSpec as P

EPS = 1e-06
MESH = pl.DeviceIdType.MESH
BF = jnp.bfloat16
F32 = jnp.float32
OWN = 8
EARLY = 6


def layer_kernel(
    experts, groups, cap,
    tokens_ref, gain_ref, routes_ref, gates_ref, wg_hbm, wu_hbm, wd_hbm, gout_ref,
    out_ref,
    wg, wu, wd, piece, column, select, slots, rows, hidden, partial, raw, terms, result, answers, comb_hi, comb_lo, squares,
    ready, w_sem, xa_s, xa_r, zs_s, zs_r, ag_s, ag_r, re_s, re_r, ra_s, ra_r, rs_s, rs_r, zr_s, zr_r, sq_s, sq_r,
):
    grp, ep, tp = lax.axis_index("grp"), lax.axis_index("ep"), lax.axis_index("tp")
    z, c = ep // 2, ep % 2
    nz = experts // 2
    count, width = tokens_ref.shape
    local_tokens = groups * count
    slice_width = width // groups
    block = groups * cap
    per_chunk = 2
    chunks = experts // per_chunk
    chunk_rows = per_chunk * block
    hidden_width = wg.shape[1]

    half = nz // 2

    def ahead(s):
        u = jnp.where(s > OWN, s - 1, s)
        mixed = jnp.where(u % 2 == 1, (u + 3) // 2, half + u // 2)
        return jnp.where(s == OWN, 0, jnp.where(u == 0, 1, mixed))

    def expert_at(s, j):
        return ((z + nz - ahead(s)) % nz) * 2 + (c + j) % 2

    def source_at(s, j):
        return ((z + ahead(s)) % nz) * 2 + (c + j) % 2

    rank_here = (ep + experts - 1) % experts

    def at_rank(r):
        return (r + 1) % experts

    def peer(j):
        return (tp + j) % groups

    def giver(j):
        return (tp + groups - j) % groups

    barrier = pltpu.get_barrier_semaphore()

    def signal(sem, device):
        pl.semaphore_signal(sem, inc=1, device_id=device, device_id_type=MESH)

    for j in range(1, groups):
        signal(barrier, (grp, ep, peer(j)))

    def greet(r, carry):
        signal(barrier, (grp, at_rank(r), tp))
        return carry

    lax.fori_loop(rank_here + 1, experts, greet, 0)

    w_copies = [
        pltpu.make_async_copy(src.at[0], dst, w_sem.at[i])
        for i, (src, dst) in enumerate(((wg_hbm, wg), (wu_hbm, wu), (wd_hbm, wd)))
    ]
    for copy in w_copies:
        copy.start()

    values = tokens_ref[...].astype(F32)
    normed = values * lax.rsqrt(jnp.mean(values * values, axis=-1, keepdims=True) + EPS) * gain_ref[...]
    normed = normed.astype(BF)
    for q in range(groups):
        piece[q] = normed[:, q * slice_width:(q + 1) * slice_width]

    at = lax.broadcasted_iota(jnp.int32, (experts, local_tokens), 0)
    expert = expert_at(at // per_chunk, at % per_chunk)
    hit0 = routes_ref[0:1, :] == expert
    hit1 = routes_ref[1:2, :] == expert
    zero = jnp.zeros((), F32)
    one = jnp.ones((), F32)
    hit = jnp.where(hit0, one, zero) + jnp.where(hit1, one, zero)
    before = (
        lax.broadcasted_iota(jnp.int32, (local_tokens, local_tokens), 0)
        < lax.broadcasted_iota(jnp.int32, (local_tokens, local_tokens), 1)
    )
    before = jnp.where(before, one, zero).astype(BF)
    rank = jnp.dot(hit.astype(BF), before, preferred_element_type=F32)
    rank = jnp.where(hit > 0, rank, -one)
    gate = jnp.where(hit0, gates_ref[0:1, :], zero) + jnp.where(hit1, gates_ref[1:2, :], zero)
    slot_of = lax.broadcasted_iota(jnp.int32, (experts, block, local_tokens), 1).astype(F32)
    chosen = rank[:, None, :] == slot_of
    select[...] = jnp.where(chosen, one, zero).reshape(experts * block, local_tokens).astype(BF)

    with jax.named_scope("entry"):
        pl.semaphore_wait(barrier, groups - 1 + rank_here)

    def answer(r, carry):
        signal(ready.at[ep], (grp, at_rank(r), tp))
        return carry

    lax.fori_loop(0, rank_here, answer, 0)

    def xa_copy(j, src, dst, device):
        return pltpu.make_async_remote_copy(
            src_ref=piece.at[src], dst_ref=column.at[dst], send_sem=xa_s.at[j - 1], recv_sem=xa_r.at[j - 1],
            device_id=(grp, ep, device), device_id_type=MESH)

    for j in range(1, groups):
        xa_copy(j, peer(j), tp, peer(j)).start()
    column[tp] = piece[tp]
    with jax.named_scope("slices"):
        for j in range(1, groups):
            xa_copy(j, peer(j), giver(j), peer(j)).wait_recv()

    def zs_copy(s, j):
        pos = s * per_chunk + j
        return pltpu.make_async_remote_copy(
            src_ref=slots.at[pos], dst_ref=rows.at[tp, pos], send_sem=zs_s.at[pos], recv_sem=zs_r.at[pos],
            device_id=(grp, expert_at(s, j), tp), device_id_type=MESH)

    def each(s, action):
        @pl.when(s != OWN)
        def _():
            action(0)

        action(1)

    def send(s, now):
        k = ahead(s)

        def one(j):
            other = expert_at(s, j)
            higher = (other + experts - 1) % experts > rank_here
            back = jnp.where((k == 0) & (other != 0), 0, (7 * (nz - k)) // 16)
            shift = jnp.where(higher, back, 0 - (7 * k) // 16)
            leave_at = jnp.minimum(jnp.maximum(s - EARLY + shift, 0), chunks - 1)

            @pl.when((leave_at == now) & higher)
            def _():
                pl.semaphore_wait(ready.at[other], 1)

            @pl.when(leave_at == now)
            def _():
                zs_copy(s, j).start()

        each(s, one)

    features = column[...].reshape(local_tokens, slice_width)

    def dispatch(k, carry):
        picked = jnp.dot(
            select[pl.ds(pl.multiple_of(k * chunk_rows, chunk_rows), chunk_rows), :],
            features, preferred_element_type=F32)
        slots[pl.ds(k * per_chunk, per_chunk)] = picked.reshape(per_chunk, block, slice_width).astype(BF)

        send(k, 0)
        return carry

    with jax.named_scope("dispatch"):
        lax.fori_loop(0, chunks, dispatch, 0)
    rows[tp, OWN * per_chunk] = slots[OWN * per_chunk]

    high = gate.astype(BF).astype(F32)
    low = gate - high
    comb_hi[...] = jnp.where(chosen, high[:, None, :], zero).reshape(experts * block, local_tokens).T.astype(BF)
    comb_lo[...] = jnp.where(chosen, low[:, None, :], zero).reshape(experts * block, local_tokens).T.astype(BF)

    with jax.named_scope("weights"):
        for copy in w_copies:
            copy.wait()

    def span(k):
        return pl.ds(k * per_chunk, per_chunk)

    def neighbour(way):
        return peer(1) if way == 0 else peer(groups - 1)

    def move(src, dst, send, recv, k, way):
        i = k * 2 + way
        return pltpu.make_async_remote_copy(
            src_ref=src, dst_ref=dst, send_sem=send.at[i], recv_sem=recv.at[i],
            device_id=(grp, ep, neighbour(way)), device_id_type=MESH)

    def ag_copy(k, way, owner):
        return move(rows.at[tp, span(k)], rows.at[owner, span(k)], ag_s, ag_r, k, way)

    def re_copy(k, way, src, dst):
        pos = k * per_chunk + way
        return move(rows.at[src, pos], rows.at[dst, pos], re_s, re_r, k, way)

    def ra_copy(k, way):
        pos = k * per_chunk + way
        return move(partial.at[peer(2), pos], raw.at[pos], ra_s, ra_r, k, way)

    def rs_copy(k, way):
        return move(partial.at[neighbour(way), span(k)], terms.at[way, span(k)], rs_s, rs_r, k, way)

    def zr_copy(k, j):
        pos = k * per_chunk + j
        return pltpu.make_async_remote_copy(
            src_ref=result.at[pos], dst_ref=answers.at[pos], send_sem=zr_s.at[pos], recv_sem=zr_r.at[pos],
            device_id=(grp, source_at(k, j), tp), device_id_type=MESH)

    def gather(k):
        with jax.named_scope("rows_wait"):
            each(k, lambda j: zs_copy(k, j).wait_recv())
        for way in range(2):
            ag_copy(k, way, tp).start()

    def relay(k):
        for way in range(2):
            with jax.named_scope("gather_wait"):
                ag_copy(k, way, neighbour(1 - way)).wait_recv()
            re_copy(k, way, neighbour(1 - way), neighbour(1 - way)).start()

    def compute(k):
        with jax.named_scope("relay_wait"):
            for way in range(2):
                re_copy(k, way, neighbour(1 - way), peer(2)).wait_recv()
        x = jnp.concatenate(
            [rows[q, span(k)].reshape(chunk_rows, slice_width) for q in range(groups)], axis=1)
        step = 256
        for n in range(hidden_width // step):
            cols = slice(n * step, (n + 1) * step)
            g = jnp.dot(x, wg[:, cols], preferred_element_type=F32)
            u = jnp.dot(x, wu[:, cols], preferred_element_type=F32)
            hidden[:, cols] = (g * (1.0 / (1.0 + jnp.exp(-g))) * u).astype(BF)
        h = hidden[...]
        for j in (2, 1, 3, 0):
            q = peer(j)
            part = jnp.dot(
                h, wd[:, pl.ds(pl.multiple_of(q * slice_width, slice_width), slice_width)],
                preferred_element_type=F32)
            partial[q, span(k)] = part.reshape(per_chunk, block, slice_width).astype(BF)
            if j == 1:
                for way in range(2):
                    ra_copy(k, way).start()

    def forward(k):
        for way in range(2):
            with jax.named_scope("raw_wait"):
                ra_copy(k, way).wait_recv()
            pos = k * per_chunk + way
            both = partial[neighbour(way), pos].astype(F32) + raw[pos].astype(F32)
            partial[neighbour(way), pos] = both.astype(BF)
        for way in range(2):
            rs_copy(k, way).start()

    def give_back(k):
        with jax.named_scope("terms_wait"):
            for way in range(2):
                rs_copy(k, way).wait_recv()
        total = partial[tp, span(k)].astype(F32)
        for way in range(2):
            total += terms[way, span(k)].astype(F32)
        result[span(k)] = total.astype(BF)
        each(k, lambda j: zr_copy(k, j).start())

    def pipeline(s, carry):
        def send_due(later, inner):
            send(later, s)
            return inner

        @pl.when((s > 0) & (s < chunks))
        def _():
            with jax.named_scope("ready_wait"):
                lax.fori_loop(0, chunks, send_due, 0)

        for lag, stage in ((6, forward), (8, give_back), (2, relay), (4, compute), (0, gather)):
            @pl.when((s >= lag) & (s < chunks + lag))
            def _(lag=lag, stage=stage):
                stage(s - lag)
        return carry

    lax.fori_loop(0, chunks + 8, pipeline, 0)
    answers[OWN * per_chunk] = result[OWN * per_chunk]

    def collect(k, carry):
        each(k, lambda j: zr_copy(k, j).wait_recv())
        return carry

    with jax.named_scope("answers_wait"):
        lax.fori_loop(0, chunks, collect, 0)
    outs = answers[...].reshape(experts * block, slice_width)
    combined = jnp.dot(comb_hi[...], outs, preferred_element_type=F32)
    combined += jnp.dot(comb_lo[...], outs, preferred_element_type=F32)

    own = jnp.sum(combined * combined, axis=1, keepdims=True)
    squares[tp] = jnp.broadcast_to(own, (local_tokens, 128)).T[:8]

    def sq_copy(j, owner):
        return pltpu.make_async_remote_copy(
            src_ref=squares.at[tp], dst_ref=squares.at[owner], send_sem=sq_s.at[j - 1], recv_sem=sq_r.at[j - 1],
            device_id=(grp, ep, peer(j)), device_id_type=MESH)

    for j in range(1, groups):
        sq_copy(j, tp).start()
    with jax.named_scope("squares_wait"):
        for j in range(1, groups):
            sq_copy(j, giver(j)).wait_recv()
    total = squares[0] + squares[1] + squares[2] + squares[3]
    scale = lax.rsqrt(total / width + EPS)
    scale = jnp.concatenate([scale] * 16, axis=0).T[:, :1]
    out_ref[...] = (combined * scale * gout_ref[...]).astype(BF)

    def drain(k, carry):
        each(k, lambda j: zs_copy(k, j).wait_send())
        each(k, lambda j: zr_copy(k, j).wait_send())
        for way in range(2):
            ag_copy(k, way, tp).wait_send()
            re_copy(k, way, tp, tp).wait_send()
            ra_copy(k, way).wait_send()
            rs_copy(k, way).wait_send()
        return carry

    with jax.named_scope("drain"):
        lax.fori_loop(0, chunks, drain, 0)
    for j in range(1, groups):
        xa_copy(j, peer(j), tp, peer(j)).wait_send()
        sq_copy(j, tp).wait_send()


def local(tokens, gain_in, routes, gates, w_gate, w_up, w_down, gain_out):
    count, width = tokens.shape
    choose = routes.shape[1]
    experts = lax.axis_size("ep")
    groups = lax.axis_size("tp")
    cap = (3 * count * choose + 2 * experts - 1) // (2 * experts)
    hidden_width = w_gate.shape[2]
    slice_width = width // groups
    block = groups * cap
    tokens_here = groups * count
    chunks = experts // 2
    vmem = pl.BlockSpec(memory_space=pltpu.VMEM)
    hbm = pl.BlockSpec(memory_space=pl.ANY)
    dma = pltpu.SemaphoreType.DMA
    return pl.pallas_call(
        functools.partial(layer_kernel, experts, groups, cap),
        out_shape=jax.ShapeDtypeStruct((tokens_here, slice_width), BF),
        in_specs=[vmem, vmem, vmem, vmem, hbm, hbm, hbm, vmem],
        out_specs=vmem,
        scratch_shapes=[
            pltpu.VMEM((width, hidden_width), BF),
            pltpu.VMEM((width, hidden_width), BF),
            pltpu.VMEM((hidden_width, width), BF),
            pltpu.VMEM((groups, count, slice_width), BF),
            pltpu.VMEM((groups, count, slice_width), BF),
            pltpu.VMEM((experts * block, tokens_here), BF),
            pltpu.VMEM((experts, block, slice_width), BF),
            pltpu.VMEM((groups, experts, block, slice_width), BF),
            pltpu.VMEM((2 * block, hidden_width), BF),
            pltpu.VMEM((groups, experts, block, slice_width), BF),
            pltpu.VMEM((experts, block, slice_width), BF),
            pltpu.VMEM((2, experts, block, slice_width), BF),
            pltpu.VMEM((experts, block, slice_width), BF),
            pltpu.VMEM((experts, block, slice_width), BF),
            pltpu.VMEM((tokens_here, experts * block), BF),
            pltpu.VMEM((tokens_here, experts * block), BF),
            pltpu.VMEM((groups, 8, tokens_here), F32),
            pltpu.SemaphoreType.REGULAR((experts,)),
            dma((3,)),
            dma((groups - 1,)), dma((groups - 1,)),
            dma((experts,)), dma((experts,)),
            *[dma((chunks * 2,)) for _ in range(8)],
            dma((experts,)), dma((experts,)),
            dma((groups - 1,)), dma((groups - 1,)),
        ],
        compiler_params=pltpu.CompilerParams(
            collective_id=0, has_side_effects=True, vmem_limit_bytes=56 * 1024 * 1024),
        name="routed_experts",
    )(tokens, gain_in.reshape(1, width), routes.T, gates.T, w_gate, w_up, w_down, gain_out.reshape(1, slice_width))


def solution(mesh):
    in_specs = (
        P(("grp", "ep", "tp"), None),
        P(),
        P(("grp", "ep"), None),
        P(("grp", "ep"), None),
        P("ep", None, "tp"),
        P("ep", None, "tp"),
        P("ep", "tp", None),
        P("tp"),
    )
    out_specs = P(("grp", "ep"), "tp")
    return jax.shard_map(local, mesh=mesh, in_specs=in_specs, out_specs=out_specs, check_vma=False)
```

time: 133 us -> 130 us (0.977)
  the two profiles are of different devices: /device:TPU:160 before, /device:TPU:33 now
where the time goes in v2:
time: 130 us; the launch traced here: 129 us
  Pallas kernels  128 us (98%)
  local copies, waits for them, and re-layouts  1.67 us (1%)
    pallas_call x1, Pallas kernels, local(): pl.pallas_call(functools.partial(layer_kernel, experts, groups, cap), out...  128 us

profile of v2, /device:TPU:33, one launch (start us, length us, event | category | flops | bytes accessed | tf_op | source)
XLA Modules:
  0.0 129.3 jit_solution(8828956459964894330)
XLA Ops:
  0.0 127.6 %routed_experts.1 = bf16[256,512]{1,0:T(8,128)(2,1)} custom-call(bf16[64,2048]{1,0:T(8,128)(2,1)} %tokens_ref.1, f32[1,2048]{1,0:T(1,128)} %bitcast.4, s32[2,256]{1,0:T(2,128)} %bitcast.5, f32[2,256]{1,0:T(2,128)} %bitcast.6, bf16[1,2048,768]{2,1,0:T(8,128)(2,1)} %wg_hbm.1, bf16[1,2048,768]{2,1,0:T(8,128)(2,1)} %wu_hbm.1, bf16[1,768,2048]{2,1,0:T(8,128)(2,1)} %wd_hbm.1, ...), custom_call_target="tpu_custom_call" | custom-call | tf_op jit(solution)/shard_map/routed_experts/pallas_call | solution.py:350
  127.6 1.7 %copy.10 = bf16[256,512]{1,0:T(8,128)(2,1)} copy(bf16[256,512]{1,0:T(8,128)(2,1)} %routed_experts.1) | data formatting | bytes 524288

commit v3 on v2

--- a/solution.py
+++ b/solution.py
@@ -11,8 +11,9 @@
 MESH = pl.DeviceIdType.MESH
 BF = jnp.bfloat16
 F32 = jnp.float32
-OWN = 8
-EARLY = 6
+OWN = 6
+NEAR = 4
+EARLY = 8
 
 
 def layer_kernel(
@@ -36,10 +37,17 @@
 
     half = nz // 2
 
+    def pick(condition, yes, no):
+        if isinstance(condition, (bool, int)):
+            return yes if condition else no
+        return jnp.where(condition, yes, no)
+
     def ahead(s):
-        u = jnp.where(s > OWN, s - 1, s)
-        mixed = jnp.where(u % 2 == 1, (u + 3) // 2, half + u // 2)
-        return jnp.where(s == OWN, 0, jnp.where(u == 0, 1, mixed))
+        u = pick(s > OWN, s - 1, s)
+        v = u - NEAR
+        mixed = pick(v % 2 == 0, half + 1 + v // 2, NEAR + (v + 1) // 2)
+        later = pick(v < 2 * (half - NEAR), mixed, u + 1)
+        return pick(s == OWN, 0, pick(u < NEAR, u + 1, later))
 
     def expert_at(s, j):
         return ((z + nz - ahead(s)) % nz) * 2 + (c + j) % 2
@@ -128,13 +136,17 @@
     def zs_copy(s, j):
         pos = s * per_chunk + j
         return pltpu.make_async_remote_copy(
-            src_ref=slots.at[pos], dst_ref=rows.at[tp, pos], send_sem=zs_s.at[pos], recv_sem=zs_r.at[pos],
+            src_ref=slots.at[pos], dst_ref=rows.at[tp, pos], send_sem=zs_s.at[0], recv_sem=zs_r.at[s],
             device_id=(grp, expert_at(s, j), tp), device_id_type=MESH)
 
     def each(s, action):
-        @pl.when(s != OWN)
-        def _():
-            action(0)
+        if isinstance(s, int):
+            if s != OWN:
+                action(0)
+        else:
+            @pl.when(s != OWN)
+            def _():
+                action(0)
 
         action(1)
 
@@ -143,17 +155,20 @@
 
         def one(j):
             other = expert_at(s, j)
-            higher = (other + experts - 1) % experts > rank_here
-            back = jnp.where((k == 0) & (other != 0), 0, (7 * (nz - k)) // 16)
-            shift = jnp.where(higher, back, 0 - (7 * k) // 16)
-            leave_at = jnp.minimum(jnp.maximum(s - EARLY + shift, 0), chunks - 1)
-
-            @pl.when((leave_at == now) & higher)
-            def _():
-                pl.semaphore_wait(ready.at[other], 1)
+            higher = (ep != 0) & ((z < k) | (other == 0) | ((k == 0) & (c == 0)))
+            behind = (7 * (nz - k)) // 16
+            behind = pick(k == 0, jnp.where(other == 0, behind, 0), behind)
+            after = jnp.maximum(jnp.maximum(s - EARLY, -2) + behind, 1)
+            before = s - EARLY - (7 * k) // 16
+            before = max(before, 0) if isinstance(s, int) else jnp.maximum(before, 0)
+            leave_at = jnp.minimum(jnp.where(higher, after, before), chunks - 1)
 
             @pl.when(leave_at == now)
             def _():
+                @pl.when(higher)
+                def _():
+                    pl.semaphore_wait(ready.at[other], 1)
+
                 zs_copy(s, j).start()
 
         each(s, one)
@@ -182,6 +197,9 @@
         for copy in w_copies:
             copy.wait()
 
+    def settle(ref, sem):
+        pltpu.make_async_copy(ref, ref, sem).wait()
+
     def span(k):
         return pl.ds(k * per_chunk, per_chunk)
 
@@ -189,9 +207,8 @@
         return peer(1) if way == 0 else peer(groups - 1)
 
     def move(src, dst, send, recv, k, way):
-        i = k * 2 + way
         return pltpu.make_async_remote_copy(
-            src_ref=src, dst_ref=dst, send_sem=send.at[i], recv_sem=recv.at[i],
+            src_ref=src, dst_ref=dst, send_sem=send.at[0], recv_sem=recv.at[k],
             device_id=(grp, ep, neighbour(way)), device_id_type=MESH)
 
     def ag_copy(k, way, owner):
@@ -211,25 +228,31 @@
     def zr_copy(k, j):
         pos = k * per_chunk + j
         return pltpu.make_async_remote_copy(
-            src_ref=result.at[pos], dst_ref=answers.at[pos], send_sem=zr_s.at[pos], recv_sem=zr_r.at[pos],
+            src_ref=result.at[pos], dst_ref=answers.at[pos], send_sem=zr_s.at[0], recv_sem=zr_r.at[0],
             device_id=(grp, source_at(k, j), tp), device_id_type=MESH)
 
     def gather(k):
         with jax.named_scope("rows_wait"):
-            each(k, lambda j: zs_copy(k, j).wait_recv())
+            @pl.when(k == OWN)
+            def _():
+                settle(rows.at[tp, k * per_chunk + 1], zs_r.at[k])
+
+            @pl.when(k != OWN)
+            def _():
+                settle(rows.at[tp, span(k)], zs_r.at[k])
+
         for way in range(2):
             ag_copy(k, way, tp).start()
 
     def relay(k):
+        with jax.named_scope("gather_wait"):
+            settle(rows.at[:2, span(k)], ag_r.at[k])
         for way in range(2):
-            with jax.named_scope("gather_wait"):
-                ag_copy(k, way, neighbour(1 - way)).wait_recv()
             re_copy(k, way, neighbour(1 - way), neighbour(1 - way)).start()
 
     def compute(k):
         with jax.named_scope("relay_wait"):
-            for way in range(2):
-                re_copy(k, way, neighbour(1 - way), peer(2)).wait_recv()
+            settle(rows.at[peer(2), span(k)], re_r.at[k])
         x = jnp.concatenate(
             [rows[q, span(k)].reshape(chunk_rows, slice_width) for q in range(groups)], axis=1)
         step = 256
@@ -250,9 +273,9 @@
                     ra_copy(k, way).start()
 
     def forward(k):
+        with jax.named_scope("raw_wait"):
+            settle(raw.at[span(k)], ra_r.at[k])
         for way in range(2):
-            with jax.named_scope("raw_wait"):
-                ra_copy(k, way).wait_recv()
             pos = k * per_chunk + way
             both = partial[neighbour(way), pos].astype(F32) + raw[pos].astype(F32)
             partial[neighbour(way), pos] = both.astype(BF)
@@ -261,8 +284,7 @@
 
     def give_back(k):
         with jax.named_scope("terms_wait"):
-            for way in range(2):
-                rs_copy(k, way).wait_recv()
+            settle(terms.at[:, span(k)], rs_r.at[k])
         total = partial[tp, span(k)].astype(F32)
         for way in range(2):
             total += terms[way, span(k)].astype(F32)
@@ -270,14 +292,11 @@
         each(k, lambda j: zr_copy(k, j).start())
 
     def pipeline(s, carry):
-        def send_due(later, inner):
-            send(later, s)
-            return inner
-
         @pl.when((s > 0) & (s < chunks))
         def _():
             with jax.named_scope("ready_wait"):
-                lax.fori_loop(0, chunks, send_due, 0)
+                for later in range(chunks):
+                    send(later, s)
 
         for lag, stage in ((6, forward), (8, give_back), (2, relay), (4, compute), (0, gather)):
             @pl.when((s >= lag) & (s < chunks + lag))
@@ -288,12 +307,8 @@
     lax.fori_loop(0, chunks + 8, pipeline, 0)
     answers[OWN * per_chunk] = result[OWN * per_chunk]
 
-    def collect(k, carry):
-        each(k, lambda j: zr_copy(k, j).wait_recv())
-        return carry
-
     with jax.named_scope("answers_wait"):
-        lax.fori_loop(0, chunks, collect, 0)
+        settle(answers.at[:experts - 1], zr_r.at[0])
     outs = answers[...].reshape(experts * block, slice_width)
     combined = jnp.dot(comb_hi[...], outs, preferred_element_type=F32)
     combined += jnp.dot(comb_lo[...], outs, preferred_element_type=F32)
@@ -316,18 +331,13 @@
     scale = jnp.concatenate([scale] * 16, axis=0).T[:, :1]
     out_ref[...] = (combined * scale * gout_ref[...]).astype(BF)
 
-    def drain(k, carry):
-        each(k, lambda j: zs_copy(k, j).wait_send())
-        each(k, lambda j: zr_copy(k, j).wait_send())
-        for way in range(2):
-            ag_copy(k, way, tp).wait_send()
-            re_copy(k, way, tp, tp).wait_send()
-            ra_copy(k, way).wait_send()
-            rs_copy(k, way).wait_send()
-        return carry
-
     with jax.named_scope("drain"):
-        lax.fori_loop(0, chunks, drain, 0)
+        settle(slots.at[:experts - 1], zs_s.at[0])
+        settle(slots.at[:experts - 1], zr_s.at[0])
+        settle(rows.at[:2], ag_s.at[0])
+        settle(slots, re_s.at[0])
+        settle(slots, ra_s.at[0])
+        settle(terms, rs_s.at[0])
     for j in range(1, groups):
         xa_copy(j, peer(j), tp, peer(j)).wait_send()
         sq_copy(j, tp).wait_send()
@@ -373,9 +383,8 @@
             pltpu.SemaphoreType.REGULAR((experts,)),
             dma((3,)),
             dma((groups - 1,)), dma((groups - 1,)),
-            dma((experts,)), dma((experts,)),
-            *[dma((chunks * 2,)) for _ in range(8)],
-            dma((experts,)), dma((experts,)),
+            *[dma((n,)) for n in (1, chunks) * 5],
+            dma((1,)), dma((1,)),
             dma((groups - 1,)), dma((groups - 1,)),
         ],
         compiler_params=pltpu.CompilerParams(

time: 130 us -> 118 us (0.908)
  Pallas kernels: 128 us -> 116 us
    pallas_call x1, Pallas kernels: 128 us -> 116 us  [local(): pl.pallas_call(functools.partial(layer_kernel, experts, groups, cap), out...]
where the time goes in v3:
time: 118 us; the launch traced here: 117 us
  Pallas kernels  116 us (98%)
  local copies, waits for them, and re-layouts  1.67 us (1%)
    pallas_call x1, Pallas kernels, local(): pl.pallas_call(functools.partial(layer_kernel, experts, groups, cap), out...  116 us

profile of v3, /device:TPU:33, one launch (start us, length us, event | category | flops | bytes accessed | tf_op | source)
XLA Modules:
  0.0 117.5 jit_solution(8565258554184627772)
XLA Ops:
  0.0 115.8 %routed_experts.1 = bf16[256,512]{1,0:T(8,128)(2,1)} custom-call(bf16[64,2048]{1,0:T(8,128)(2,1)} %tokens_ref.1, f32[1,2048]{1,0:T(1,128)} %bitcast.4, s32[2,256]{1,0:T(2,128)} %bitcast.5, f32[2,256]{1,0:T(2,128)} %bitcast.6, bf16[1,2048,768]{2,1,0:T(8,128)(2,1)} %wg_hbm.1, bf16[1,2048,768]{2,1,0:T(8,128)(2,1)} %wu_hbm.1, bf16[1,768,2048]{2,1,0:T(8,128)(2,1)} %wd_hbm.1, ...), custom_call_target="tpu_custom_call" | custom-call | tf_op jit(solution)/shard_map/routed_experts/pallas_call | solution.py:360
  115.8 1.7 %copy.10 = bf16[256,512]{1,0:T(8,128)(2,1)} copy(bf16[256,512]{1,0:T(8,128)(2,1)} %routed_experts.1) | data formatting | bytes 524288

commit v4 on v3

--- a/solution.py
+++ b/solution.py
@@ -11,9 +11,8 @@
 MESH = pl.DeviceIdType.MESH
 BF = jnp.bfloat16
 F32 = jnp.float32
-OWN = 6
 NEAR = 4
-EARLY = 8
+EARLY = 6
 
 
 def layer_kernel(
@@ -36,24 +35,29 @@
     hidden_width = wg.shape[1]
 
     half = nz // 2
-
-    def pick(condition, yes, no):
-        if isinstance(condition, (bool, int)):
-            return yes if condition else no
-        return jnp.where(condition, yes, no)
-
-    def ahead(s):
-        u = pick(s > OWN, s - 1, s)
-        v = u - NEAR
-        mixed = pick(v % 2 == 0, half + 1 + v // 2, NEAR + (v + 1) // 2)
-        later = pick(v < 2 * (half - NEAR), mixed, u + 1)
-        return pick(s == OWN, 0, pick(u < NEAR, u + 1, later))
-
-    def expert_at(s, j):
-        return ((z + nz - ahead(s)) % nz) * 2 + (c + j) % 2
-
-    def source_at(s, j):
-        return ((z + ahead(s)) % nz) * 2 + (c + j) % 2
+    ends = [k for i in range(1, NEAR) for k in (nz - i, i)] + [0]
+    middle = [NEAR] + [k for i in range(NEAR, half - 1) for k in (nz - i, i + 1)] + [half + 1, half]
+    order_low = list(range(1, NEAR + 1)) + [0, NEAR + 1] + list(range(nz - NEAR + 1, nz)) + middle[3:] + middle[1:2]
+    order_low = [k for i, k in enumerate(order_low) if k not in order_low[:i]]
+    order_mid = ends + middle
+    order_high = ends + middle[::-1]
+
+    def by_place(chip, low, mid, high):
+        return jnp.where(chip < NEAR, low, jnp.where(chip < half, mid, high))
+
+    here = [by_place(z, *ks) for ks in zip(order_low, order_mid, order_high)]
+
+    def part_at(s):
+        k = here[0]
+        for i in range(1, nz):
+            k = jnp.where(s == i, here[i], k)
+        return k
+
+    def expert_at(k, j):
+        return ((z + nz - k) % nz) * 2 + (c + j) % 2
+
+    def source_at(k, j):
+        return ((z + k) % nz) * 2 + (c + j) % 2
 
     rank_here = (ep + experts - 1) % experts
 
@@ -133,34 +137,31 @@
         for j in range(1, groups):
             xa_copy(j, peer(j), giver(j), peer(j)).wait_recv()
 
-    def zs_copy(s, j):
-        pos = s * per_chunk + j
+    def zs_copy(k, j):
+        pos = k * per_chunk + j
         return pltpu.make_async_remote_copy(
-            src_ref=slots.at[pos], dst_ref=rows.at[tp, pos], send_sem=zs_s.at[0], recv_sem=zs_r.at[s],
-            device_id=(grp, expert_at(s, j), tp), device_id_type=MESH)
-
-    def each(s, action):
-        if isinstance(s, int):
-            if s != OWN:
+            src_ref=slots.at[pos], dst_ref=rows.at[tp, pos], send_sem=zs_s.at[0], recv_sem=zs_r.at[k],
+            device_id=(grp, expert_at(k, j), tp), device_id_type=MESH)
+
+    def each(k, action):
+        if isinstance(k, int):
+            if k != 0:
                 action(0)
         else:
-            @pl.when(s != OWN)
+            @pl.when(k != 0)
             def _():
                 action(0)
 
         action(1)
 
-    def send(s, now):
-        k = ahead(s)
-
+    def send(k, now):
         def one(j):
-            other = expert_at(s, j)
+            other = expert_at(k, j)
+            step = by_place(other // 2, order_low.index(k), order_mid.index(k), order_high.index(k))
             higher = (ep != 0) & ((z < k) | (other == 0) | ((k == 0) & (c == 0)))
-            behind = (7 * (nz - k)) // 16
-            behind = pick(k == 0, jnp.where(other == 0, behind, 0), behind)
-            after = jnp.maximum(jnp.maximum(s - EARLY, -2) + behind, 1)
-            before = s - EARLY - (7 * k) // 16
-            before = max(before, 0) if isinstance(s, int) else jnp.maximum(before, 0)
+            apart = jnp.where(other == 0, nz, 0) if k == 0 else nz - k
+            after = jnp.maximum(step - EARLY + (7 * apart) // 16, jnp.clip((apart - 2) // 2, 0, 4))
+            before = jnp.maximum(step - EARLY - (7 * k) // 16, 0)
             leave_at = jnp.minimum(jnp.where(higher, after, before), chunks - 1)
 
             @pl.when(leave_at == now)
@@ -169,24 +170,20 @@
                 def _():
                     pl.semaphore_wait(ready.at[other], 1)
 
-                zs_copy(s, j).start()
-
-        each(s, one)
+                zs_copy(k, j).start()
+
+        each(k, one)
 
     features = column[...].reshape(local_tokens, slice_width)
 
-    def dispatch(k, carry):
-        picked = jnp.dot(
-            select[pl.ds(pl.multiple_of(k * chunk_rows, chunk_rows), chunk_rows), :],
-            features, preferred_element_type=F32)
-        slots[pl.ds(k * per_chunk, per_chunk)] = picked.reshape(per_chunk, block, slice_width).astype(BF)
-
-        send(k, 0)
-        return carry
-
+    by_distance = [0] + [k for i in range(1, half) for k in (i, nz - i)] + [half]
     with jax.named_scope("dispatch"):
-        lax.fori_loop(0, chunks, dispatch, 0)
-    rows[tp, OWN * per_chunk] = slots[OWN * per_chunk]
+        for k in by_distance:
+            picked = jnp.dot(
+                select[k * chunk_rows:(k + 1) * chunk_rows, :], features, preferred_element_type=F32)
+            slots[k * per_chunk:(k + 1) * per_chunk] = picked.reshape(per_chunk, block, slice_width).astype(BF)
+            send(k, 0)
+    rows[tp, 0] = slots[0]
 
     high = gate.astype(BF).astype(F32)
     low = gate - high
@@ -233,11 +230,11 @@
 
     def gather(k):
         with jax.named_scope("rows_wait"):
-            @pl.when(k == OWN)
+            @pl.when(k == 0)
             def _():
                 settle(rows.at[tp, k * per_chunk + 1], zs_r.at[k])
 
-            @pl.when(k != OWN)
+            @pl.when(k != 0)
             def _():
                 settle(rows.at[tp, span(k)], zs_r.at[k])
 
@@ -295,17 +292,17 @@
         @pl.when((s > 0) & (s < chunks))
         def _():
             with jax.named_scope("ready_wait"):
-                for later in range(chunks):
-                    send(later, s)
+                for k in by_distance:
+                    send(k, s)
 
         for lag, stage in ((6, forward), (8, give_back), (2, relay), (4, compute), (0, gather)):
             @pl.when((s >= lag) & (s < chunks + lag))
             def _(lag=lag, stage=stage):
-                stage(s - lag)
+                stage(part_at(s - lag))
         return carry
 
     lax.fori_loop(0, chunks + 8, pipeline, 0)
-    answers[OWN * per_chunk] = result[OWN * per_chunk]
+    answers[0] = result[0]
 
     with jax.named_scope("answers_wait"):
         settle(answers.at[:experts - 1], zr_r.at[0])

time: 118 us -> 117 us (level)
  no operation moved by 1% of the time
where the time goes in v4:
time: 117 us; the launch traced here: 116 us
  Pallas kernels  115 us (98%)
  local copies, waits for them, and re-layouts  1.67 us (1%)
    pallas_call x1, Pallas kernels, local(): pl.pallas_call(functools.partial(layer_kernel, experts, groups, cap), out...  115 us

profile of v4, /device:TPU:33, one launch (start us, length us, event | category | flops | bytes accessed | tf_op | source)
XLA Modules:
  0.0 116.4 jit_solution(13553995528476190783)
XLA Ops:
  0.0 114.7 %routed_experts.1 = bf16[256,512]{1,0:T(8,128)(2,1)} custom-call(bf16[64,2048]{1,0:T(8,128)(2,1)} %tokens_ref.1, f32[1,2048]{1,0:T(1,128)} %bitcast.4, s32[2,256]{1,0:T(2,128)} %bitcast.5, f32[2,256]{1,0:T(2,128)} %bitcast.6, bf16[1,2048,768]{2,1,0:T(8,128)(2,1)} %wg_hbm.1, bf16[1,2048,768]{2,1,0:T(8,128)(2,1)} %wu_hbm.1, bf16[1,768,2048]{2,1,0:T(8,128)(2,1)} %wd_hbm.1, ...), custom_call_target="tpu_custom_call" | custom-call | tf_op jit(solution)/shard_map/routed_experts/pallas_call | solution.py:357
  114.7 1.7 %copy.10 = bf16[256,512]{1,0:T(8,128)(2,1)} copy(bf16[256,512]{1,0:T(8,128)(2,1)} %routed_experts.1) | data formatting | bytes 524288

commit v5 on v4

--- a/solution.py
+++ b/solution.py
@@ -12,7 +12,7 @@
 BF = jnp.bfloat16
 F32 = jnp.float32
 NEAR = 4
-EARLY = 6
+EARLY = 5
 
 
 def layer_kernel(
@@ -160,7 +160,8 @@
             step = by_place(other // 2, order_low.index(k), order_mid.index(k), order_high.index(k))
             higher = (ep != 0) & ((z < k) | (other == 0) | ((k == 0) & (c == 0)))
             apart = jnp.where(other == 0, nz, 0) if k == 0 else nz - k
-            after = jnp.maximum(step - EARLY + (7 * apart) // 16, jnp.clip((apart - 2) // 2, 0, 4))
+            latest = jnp.where(other == 0, 3, 4) if 0 < k < NEAR else 4
+            after = jnp.maximum(step - EARLY + (7 * apart) // 16, jnp.clip((apart - 2) // 2, 0, latest))
             before = jnp.maximum(step - EARLY - (7 * k) // 16, 0)
             leave_at = jnp.minimum(jnp.where(higher, after, before), chunks - 1)
 

time: 117 us -> 114 us (0.974)
  Pallas kernels: 115 us -> 112 us
    pallas_call x1, Pallas kernels: 115 us -> 112 us  [local(): pl.pallas_call(functools.partial(layer_kernel, experts, groups, cap), out...]
where the time goes in v5:
time: 114 us
  Pallas kernels  112 us (98%)
  local copies, waits for them, and re-layouts  1.67 us (1%)
    pallas_call x1, Pallas kernels, local(): pl.pallas_call(functools.partial(layer_kernel, experts, groups, cap), out...  112 us

profile of v5, /device:TPU:33, one launch (start us, length us, event | category | flops | bytes accessed | tf_op | source)
XLA Modules:
  0.0 114.2 jit_solution(3673227580419458212)
XLA Ops:
  0.0 112.5 %routed_experts.1 = bf16[256,512]{1,0:T(8,128)(2,1)} custom-call(bf16[64,2048]{1,0:T(8,128)(2,1)} %tokens_ref.1, f32[1,2048]{1,0:T(1,128)} %bitcast.4, s32[2,256]{1,0:T(2,128)} %bitcast.5, f32[2,256]{1,0:T(2,128)} %bitcast.6, bf16[1,2048,768]{2,1,0:T(8,128)(2,1)} %wg_hbm.1, bf16[1,2048,768]{2,1,0:T(8,128)(2,1)} %wu_hbm.1, bf16[1,768,2048]{2,1,0:T(8,128)(2,1)} %wd_hbm.1, ...), custom_call_target="tpu_custom_call" | custom-call | tf_op jit(solution)/shard_map/routed_experts/pallas_call | solution.py:358
  112.5 1.7 %copy.10 = bf16[256,512]{1,0:T(8,128)(2,1)} copy(bf16[256,512]{1,0:T(8,128)(2,1)} %routed_experts.1) | data formatting | bytes 524288
